TPU v7x, 32 devices: a whole 2x2x4 slice. The times are simulated.
32 devices in a mesh: sp: 8 (over z, y), dp: 4 (over x, core).
Axes of the slice: x: 2, y: 2, z: 4, core: 2. Of those that a mesh axis runs over, the one named last changes fastest.
Arguments:
- queries: bfloat16 [4, 1024, 16, 128], P('dp', 'sp'), may hold values from -7 to 7
- key_vectors: bfloat16 [4, 1024, 16, 128], P('dp', 'sp'), may hold values from -6 to 6
- value_vectors: bfloat16 [4, 1024, 16, 128], P('dp', 'sp'), may hold values from -6 to 6
- head_lambda: float32 [16], P('sp'), may hold values from 0.3 to 0.8
- head_gain: float32 [128], replicated, may hold values from 0.1 to 1.9
- residual: bfloat16 [4, 1024, 2048], P('dp', 'sp'), may hold values from -6 to 6
- out_weight: bfloat16 [2048, 2048], replicated, may hold values from -0.125 to 0.125
- mix_gain: float32 [2048], replicated, may hold values from 0.1 to 1.9
- pre_gain: float32 [2048], replicated, may hold values from 0.1 to 1.9
- post_gain: float32 [2048], replicated, may hold values from 0.1 to 1.9
- routes: int32 [4, 1024, 4], P('dp', 'sp'), may hold values from 0 to 31, all different within a row; in each aligned block of 128 rows (0 to 127, 128 to 255, ..., all dimensions but the last counted through in order) at most 24 rows name the same one
- route_weights: float32 [4, 1024, 4], P('dp', 'sp'), may hold values from 0.25 to 1
- expert_gate: bfloat16 [32, 2048, 512], P(('sp', 'dp')), may hold values from -0.125 to 0.125
- expert_up: bfloat16 [32, 2048, 512], P(('sp', 'dp')), may hold values from -0.125 to 0.125
- expert_down: bfloat16 [32, 512, 2048], P(('sp', 'dp')), may hold values from -0.25 to 0.25
- shared_gate: bfloat16 [2048, 512], replicated, may hold values from -0.125 to 0.125
- shared_up: bfloat16 [2048, 512], replicated, may hold values from -0.125 to 0.125
- shared_down: bfloat16 [512, 2048], replicated, may hold values from -0.25 to 0.25
Outputs:
- output: bfloat16 [4, 1024, 2048], P('dp', 'sp')
Inputs may be any that keep to these rules, and one draw needn't show every extreme that they name: `routes`: among the tokens of one device (aligned blocks of 128 positions), no expert is named more than 24 times; in some block some expert is named exactly 24 times. Each token names 4 different experts.
All inputs are finite; a program needn't handle non-finite values.
Results may differ from a plain program's by a relative error of at most 0.0075.
Values may be sent and summed in bfloat16 or wider, within the bound.
A program may use at most 128 MiB of HBM per device.

v0:
```python
import jax
import jax.numpy as jnp
from jax import lax
from jax.sharding import PartitionSpec as P

epsilon = 1e-06


def rms_scale(values_in, gain):
    return (
        values_in
        * lax.rsqrt(jnp.mean(values_in * values_in, axis=-1, keepdims=True) + epsilon)
        * gain
    )


def feed_forward(rows, gate_w, up_w, down_w):
    gate_val = jnp.dot(rows, gate_w, preferred_element_type=jnp.float32)
    up_val = jnp.dot(rows, up_w, preferred_element_type=jnp.float32)
    hidden = (jax.nn.silu(gate_val) * up_val).astype(jnp.bfloat16)
    return jnp.dot(hidden, down_w, preferred_element_type=jnp.float32).astype(jnp.bfloat16)


def attend_heads(query_heads, key_heads, value_heads, head_lambda, head_gain):
    length = query_heads.shape[0]
    head_count = query_heads.shape[1]
    head_size = query_heads.shape[2] // 2
    block_rows = min(512, length)
    block_count = length // block_rows
    query_blocks = query_heads.reshape(block_count, block_rows, head_count, 2, head_size)
    key_all = key_heads.reshape(length, head_count, 2, head_size)
    key_pos = jnp.arange(length, dtype=jnp.int32)

    def one_block(inputs):
        query_block, block_index = inputs
        scores = jnp.einsum(
            "qhmd,khmd->hmqk", query_block, key_all, preferred_element_type=jnp.float32
        ) * head_size ** (-0.5)
        query_pos = block_index * block_rows + jnp.arange(block_rows, dtype=jnp.int32)
        causal = key_pos[None, :] <= query_pos[:, None]
        scores = jnp.where(causal, scores, -jnp.inf)
        maxima = jnp.max(scores, axis=-1, keepdims=True)
        exponent = jnp.exp(scores - maxima)
        softmax_both = exponent / jnp.sum(exponent, axis=-1, keepdims=True)
        mixture = (softmax_both[:, 0] - head_lambda[:, None, None] * softmax_both[:, 1]).astype(
            jnp.bfloat16
        )
        head_output = jnp.einsum(
            "hqk,khe->qhe", mixture, value_heads, preferred_element_type=jnp.float32
        )
        return rms_scale(head_output, head_gain).astype(jnp.bfloat16)

    outputs = lax.map(one_block, (query_blocks, jnp.arange(block_count, dtype=jnp.int32)))
    return outputs.reshape(length, head_count, -1)


def local(
    queries,
    key_vectors,
    value_vectors,
    head_lambda,
    head_gain,
    residual,
    out_weight,
    mix_gain,
    pre_gain,
    post_gain,
    routes,
    route_weights,
    expert_gate,
    expert_up,
    expert_down,
    shared_gate,
    shared_up,
    shared_down,
):
    query_heads, key_heads, value_heads = (
        lax.all_to_all(queries[0], "sp", split_axis=1, concat_axis=0, tiled=True),
        lax.all_to_all(key_vectors[0], "sp", split_axis=1, concat_axis=0, tiled=True),
        lax.all_to_all(value_vectors[0], "sp", split_axis=1, concat_axis=0, tiled=True),
    )
    attended = attend_heads(query_heads, key_heads, value_heads, head_lambda, head_gain)
    token_heads = lax.all_to_all(attended, "sp", split_axis=0, concat_axis=1, tiled=True)
    tok_count = token_heads.shape[0]
    flat_heads = token_heads.reshape(tok_count, -1)
    mixed_rows = jnp.dot(flat_heads, out_weight, preferred_element_type=jnp.float32)
    updated = (residual[0].astype(jnp.float32) + rms_scale(mixed_rows, mix_gain)).astype(
        jnp.bfloat16
    )
    normed = rms_scale(updated.astype(jnp.float32), pre_gain).astype(jnp.bfloat16)
    model_width = normed.shape[1]
    experts_total = lax.axis_size("sp") * lax.axis_size("dp")
    top_count = routes.shape[2]
    capacity = 3 * tok_count * top_count // (2 * experts_total)
    assign_count = tok_count * top_count
    flat_routes = routes[0].reshape(assign_count)
    one_hot = (flat_routes[:, None] == jnp.arange(experts_total, dtype=jnp.int32)[None, :]).astype(
        jnp.int32
    )
    earlier = jnp.cumsum(one_hot, axis=0) - one_hot
    rank_index = jnp.sum(earlier * one_hot, axis=1)
    slot_index = flat_routes * capacity + rank_index
    source_row = (
        jnp.zeros((experts_total * capacity,), jnp.int32)
        .at[slot_index]
        .set(jnp.arange(assign_count, dtype=jnp.int32) // top_count)
    )
    occupied = (
        jnp.zeros((experts_total * capacity,), jnp.bfloat16)
        .at[slot_index]
        .set(jnp.ones((assign_count,), jnp.bfloat16))
    )
    outgoing = (normed[source_row] * occupied[:, None]).reshape(
        experts_total, capacity, model_width
    )
    shared_out = feed_forward(normed, shared_gate, shared_up, shared_down)
    arrived = lax.all_to_all(outgoing, ("sp", "dp"), split_axis=0, concat_axis=0, tiled=True)
    flat_rows = arrived.reshape(-1, model_width)
    result_rows = feed_forward(flat_rows, expert_gate[0], expert_up[0], expert_down[0])
    results = result_rows.reshape(arrived.shape[0], -1, model_width)
    returned = lax.all_to_all(results, ("sp", "dp"), split_axis=0, concat_axis=0, tiled=True)
    picked = returned.reshape(experts_total * capacity, model_width)[slot_index]
    routed = jnp.sum(
        picked.astype(jnp.float32).reshape(tok_count, top_count, model_width)
        * route_weights[0][:, :, None],
        axis=1,
    )
    combined = routed + shared_out.astype(jnp.float32)
    output = (updated.astype(jnp.float32) + rms_scale(combined, post_gain)).astype(jnp.bfloat16)
    return output.reshape(1, tok_count, model_width)


def solution(mesh):
    in_specs = (
        P("dp", "sp", None, None),
        P("dp", "sp", None, None),
        P("dp", "sp", None, None),
        P("sp"),
        P(),
        P("dp", "sp", None),
        P(),
        P(),
        P(),
        P(),
        P("dp", "sp", None),
        P("dp", "sp", None),
        P(("sp", "dp"), None, None),
        P(("sp", "dp"), None, None),
        P(("sp", "dp"), None, None),
        P(),
        P(),
        P(),
    )
    out_specs = P("dp", "sp", None)
    return jax.shard_map(local, mesh=mesh, in_specs=in_specs, out_specs=out_specs, check_vma=False)
```

profile of v0, /device:TPU:0, one launch (start us, length us, event | category | flops | bytes accessed | tf_op | source)
XLA Modules:
  0.0 313.4 jit_solution(17790925592510892741)
XLA Ops:
  0.0 2.1 copy.77
  2.1 7.3 %all-to-all-start = ((bf16[128,16,128]{2,0,1:T(8,128)(2,1)}), bf16[128,16,128]{2,0,1:T(8,128)(2,1)S(1)}, u32[]{:S(2)}, u32[]{:S(2)}) async-start(bf16[128,16,128]{2,0,1:T(8,128)(2,1)} %bitcast.132), calls=%async_computation | async-start | bytes 1048576 | tf_op jit(solution)/shard_map/all_to_all | solution.py:78
  9.4 2.0 copy.75
  11.4 12.5 %all-to-all-done = bf16[128,16,128]{2,0,1:T(8,128)(2,1)S(1)} async-done(((bf16[128,16,128]{2,0,1:T(8,128)(2,1)}), bf16[128,16,128]{2,0,1:T(8,128)(2,1)S(1)}, u32[]{:S(2)}, u32[]{:S(2)}) %all-to-all-start) | async-done | bytes 524320 | tf_op jit(solution)/shard_map/all_to_all | solution.py:78
  23.9 3.6 %all-to-all-start.2 = ((bf16[128,16,128]{2,0,1:T(8,128)(2,1)}), bf16[128,16,128]{2,0,1:T(8,128)(2,1)S(1)}, u32[]{:S(2)}, u32[]{:S(2)}) async-start(bf16[128,16,128]{2,0,1:T(8,128)(2,1)} %bitcast.155), calls=%async_computation.2 | async-start | bytes 1048576 | tf_op jit(solution)/shard_map/all_to_all | solution.py:80
  29.5 12.7 %all-to-all-done.2 = bf16[128,16,128]{2,0,1:T(8,128)(2,1)S(1)} async-done(((bf16[128,16,128]{2,0,1:T(8,128)(2,1)}), bf16[128,16,128]{2,0,1:T(8,128)(2,1)S(1)}, u32[]{:S(2)}, u32[]{:S(2)}) %all-to-all-start.2) | async-done | bytes 524320 | tf_op jit(solution)/shard_map/all_to_all | solution.py:80
  42.2 4.1 %all-to-all-start.1 = ((bf16[128,16,128]{2,0,1:T(8,128)(2,1)}), bf16[128,16,128]{2,0,1:T(8,128)(2,1)}, u32[]{:S(2)}, u32[]{:S(2)}) async-start(bf16[128,16,128]{2,0,1:T(8,128)(2,1)} %bitcast.154), calls=%async_computation.1 | async-start | bytes 1048576 | tf_op jit(solution)/shard_map/all_to_all | solution.py:79
  52.8 7.8 %all-to-all-done.1 = bf16[128,16,128]{2,0,1:T(8,128)(2,1)} async-done(((bf16[128,16,128]{2,0,1:T(8,128)(2,1)}), bf16[128,16,128]{2,0,1:T(8,128)(2,1)}, u32[]{:S(2)}, u32[]{:S(2)}) %all-to-all-start.1) | async-done | bytes 524320 | tf_op jit(solution)/shard_map/all_to_all | solution.py:79
  63.1 29.6 %while.11 = (s32[]{:T(128)}, bf16[2,512,2,128]{3,1,0,2:T(8,128)(2,1)}, s32[2]{0:T(128)S(1)}, bf16[2,512,2,2,64]{1,4,3,2,0:T(8,128)(2,1)S(1)}, bf16[1024,2,2,64]{...) while((s32[]{:T(128)}, ...), condition=%wide.region_4.5_spmd.clone, body=%wide.region_0.4_spmd.clone.sunk | while | flops 551684608 | bytes 40408232 | solution.py:53
  64.9 7.1 %fusion.99 = (f32[2,2,512]{2,1,0:T(2,128)S(1)}, f32[2,2,512,1024]{3,2,1,0:T(8,128)}) fusion(pred[512,1024]{1,0:T(8,128)(4,1)S(1)} %iota_compare_fusion.4, bf16[1024,2,2,64]{0,3,2,1:T(8,128)(2,1)} %get-tuple-element.202, bf16[2,512,2,2,64]{1,4,3,2,0:T(8,128)(2,1)S(1)} %get-tuple-element.201, s32[]{:T(128)} %get-tuple-element.188), kind=kOutput, calls=%fused_computation.102.clone.1 | convolution fusion | flops 276825088 | bytes 9707524 | tf_op jit(solution)/shard_map/while/body/eval_jaxpr/sub | solution.py:43
  72.0 4.0 %broadcast_divide_fusion.2 = f32[2,2,512,1024]{3,2,1,0:T(8,128)S(1)} fusion(f32[2,2,512,1024]{3,2,1,0:T(8,128)} %get-tuple-element.174, f32[2,2,512]{2,1,0:T(2,128)S(1)} %get-tuple-element.175), kind=kLoop, calls=%fused_computation.14.clone.1 | loop fusion | flops 2097152 | bytes 16785408 | tf_op jit(solution)/shard_map/while/body/eval_jaxpr/div | solution.py:44
  79.7 7.1 %fusion.99 = (f32[2,2,512]{2,1,0:T(2,128)S(1)}, f32[2,2,512,1024]{3,2,1,0:T(8,128)}) fusion(pred[512,1024]{1,0:T(8,128)(4,1)S(1)} %iota_compare_fusion.4, bf16[1024,2,2,64]{0,3,2,1:T(8,128)(2,1)} %get-tuple-element.202, bf16[2,512,2,2,64]{1,4,3,2,0:T(8,128)(2,1)S(1)} %get-tuple-element.201, s32[]{:T(128)} %get-tuple-element.188), kind=kOutput, calls=%fused_computation.102.clone.1 | convolution fusion | flops 276825088 | bytes 9707524 | tf_op jit(solution)/shard_map/while/body/eval_jaxpr/sub | solution.py:43
  86.8 4.0 %broadcast_divide_fusion.2 = f32[2,2,512,1024]{3,2,1,0:T(8,128)S(1)} fusion(f32[2,2,512,1024]{3,2,1,0:T(8,128)} %get-tuple-element.174, f32[2,2,512]{2,1,0:T(2,128)S(1)} %get-tuple-element.175), kind=kLoop, calls=%fused_computation.14.clone.1 | loop fusion | flops 2097152 | bytes 16785408 | tf_op jit(solution)/shard_map/while/body/eval_jaxpr/div | solution.py:44
  92.7 2.4 copy.59
  95.1 3.6 %all-to-all-start.3 = ((bf16[1024,2,128]{2,1,0:T(2,128)(2,1)}), bf16[1024,2,128]{2,1,0:T(2,128)(2,1)S(1)}, u32[]{:S(2)}, u32[]{:S(2)}) async-start(bf16[1024,2,128]{2,1,0:T(2,128)(2,1)} %copy.59), calls=%async_computation.3 | async-start | bytes 1048576 | tf_op jit(solution)/shard_map/all_to_all | solution.py:83
  99.1 2.6 scatter_custom_fusion
  101.7 3.8 %scatter_custom_fusion.1 = bf16[768]{0:T(1024)(128)(2,1)S(1)} fusion(s32[512]{0:T(512)S(1)} %bitcast.160, bf16[512]{0:T(512)(128)(2,1)S(1)} %broadcast.140, bf16[]{:T(256)} %constant.60.clone.1), kind=kCustom, calls=%fused_computation.94 | custom fusion | bytes 1538 | tf_op jit(solution)/shard_map/scatter | solution.py:111
  105.6 7.6 %all-to-all-done.3 = bf16[1024,2,128]{2,1,0:T(2,128)(2,1)S(1)} async-done(((bf16[1024,2,128]{2,1,0:T(2,128)(2,1)}), bf16[1024,2,128]{2,1,0:T(2,128)(2,1)S(1)}, u32[]{:S(2)}, u32[]{:S(2)}) %all-to-all-start.3) | async-done | bytes 524320 | tf_op jit(solution)/shard_map/all_to_all | solution.py:83
  113.7 4.8 %multiply_reduce_fusion.3 = (f32[128]{0:T(128)S(1)}, f32[128,2048]{1,0:T(8,128)S(1)}) fusion(bf16[128,2048]{0,1:T(8,128)(2,1)S(1)} %bitcast.148, bf16[2048,2048]{1,0:T(8,128)(2,1)} %param.26), kind=kOutput, calls=%fused_computation.61 | convolution fusion | flops 1074265984 | bytes 9961984 | tf_op jit(solution)/shard_map/dot_general | solution.py:86
  119.1 4.3 %gather_fusion = bf16[768,2048]{1,0:T(8,128)(2,1)} fusion(bf16[128,2048]{1,0:T(8,128)(2,1)S(1)} %fusion.47, s32[1024]{0:T(1024)S(1)} %pad_clamp_fusion.1), kind=kCustom, calls=%fused_computation | custom fusion | bytes 6294528 | tf_op jit(solution)/shard_map/gather | solution.py:113
  123.4 2.2 broadcast_multiply_fusion
  125.5 74.6 %all_to_all.73 = bf16[32,24,2048]{2,1,0:T(8,128)(2,1)S(1)} all-to-all(bf16[32,24,2048]{2,1,0:T(8,128)(2,1)S(1)} %broadcast_multiply_fusion), channel_id=1, replica_groups=mesh['sp'=8,'dp'=4] {'sp','dp'}, dimensions={0} | all-to-all | bytes 6291456 | tf_op jit(solution)/shard_map/all_to_all | solution.py:117
  201.8 2.9 fusion.40
  204.8 8.1 %convolution_convert_fusion = bf16[768,2048]{1,0:T(8,128)(2,1)} fusion(bf16[1,512,2048]{2,1,0:T(8,128)(2,1)S(1)} %copy-done, f32[768,512]{1,0:T(8,128)} %fusion.40, bf16[768,2048]{1,0:T(8,128)(2,1)} %bitcast.151, bf16[1,2048,512]{2,1,0:T(8,128)(2,1)} %param.33), kind=kOutput, calls=%fused_computation.38 | convolution fusion | flops 3225157632 | bytes 12058624 | tf_op jit(solution)/shard_map/dot_general | solution.py:21
  212.9 4.0 %all-to-all-start.5 = ((bf16[32,24,2048]{2,1,0:T(8,128)(2,1)}), bf16[32,24,2048]{2,1,0:T(8,128)(2,1)}, u32[]{:S(2)}, u32[]{:S(2)}) async-start(bf16[32,24,2048]{2,1,0:T(8,128)(2,1)} %bitcast.149), calls=%async_computation.5 | async-start | bytes 6291456 | tf_op jit(solution)/shard_map/all_to_all | solution.py:121
  217.1 2.0 fusion.78
  219.1 69.1 %all-to-all-done.5 = bf16[32,24,2048]{2,1,0:T(8,128)(2,1)} async-done(((bf16[32,24,2048]{2,1,0:T(8,128)(2,1)}), bf16[32,24,2048]{2,1,0:T(8,128)(2,1)}, u32[]{:S(2)}, u32[]{:S(2)}) %all-to-all-start.5) | async-done | bytes 3145760 | tf_op jit(solution)/shard_map/all_to_all | solution.py:121
  288.2 7.5 %gather_fusion.1 = bf16[512,2048]{1,0:T(8,128)(2,1)} fusion(bf16[768,2048]{1,0:T(8,128)(2,1)} %bitcast.23, s32[1024]{0:T(1024)S(1)} %pad_clamp_fusion), kind=kCustom, calls=%fused_computation.1 | custom fusion | bytes 4196352 | tf_op jit(solution)/shard_map/gather | solution.py:122
  295.7 4.8 %reshape.143 = f32[128,4,2048]{2,1,0:T(4,128)} reshape(bf16[512,2048]{1,0:T(8,128)(2,1)} %gather_fusion.1) | data formatting | bytes 6291456 | tf_op jit(solution)/shard_map/convert_element_type | solution.py:124
  300.4 6.3 %multiply_reduce_fusion.1 = f32[128,2048]{1,0:T(8,128)} fusion(f32[128,4,2048]{2,1,0:T(4,128)} %reshape.143, f32[128,4]{1,0:T(8,128)S(1)} %copy.66), kind=kLoop, calls=%fused_computation.37 | loop fusion | flops 1835008 | bytes 5244928 | tf_op jit(solution)/shard_map/reduce_sum | solution.py:123
  306.8 4.3 %multiply_reduce_fusion.2 = (f32[128]{0:T(128)S(1)}, f32[128,2048]{1,0:T(8,128)}) fusion(f32[128,2048]{1,0:T(8,128)} %multiply_reduce_fusion.1, bf16[512,2048]{1,0:T(8,128)(2,1)} %param.37, bf16[128,2048]{1,0:T(8,128)(2,1)S(1)} %fusion.47, bf16[2048,512]{1,0:T(8,128)(2,1)} %param.36, f32[128,512]{1,0:T(8,128)S(1)} %fusion.78), kind=kOutput, calls=%fused_computation.60 | convolution fusion | flops 538574720 | bytes 7078400 | tf_op jit(solution)/shard_map/dot_general | solution.py:21
  311.1 2.2 fusion.52
  (84 shorter events, 20.0 us)
Async XLA Ops:
  0.0 204.8 %copy-start = (bf16[1,512,2048]{2,1,0:T(8,128)(2,1)S(1)}, bf16[1,512,2048]{2,1,0:T(8,128)(2,1)}, u32[]{:S(2)}) copy-start(bf16[1,512,2048]{2,1,0:T(8,128)(2,1)} %param.34) | copy-start | bytes 6291460
  0.0 46.4 %copy-start.10 = (s32[1,128,4]{1,2,0:T(4,128)S(1)}, s32[1,128,4]{1,2,0:T(4,128)}, u32[]{:S(2)}) copy-start(s32[1,128,4]{1,2,0:T(4,128)} %param.30) | copy-start | bytes 6148
  2.1 21.8 %all-to-all-start = ((bf16[128,16,128]{2,0,1:T(8,128)(2,1)}), bf16[128,16,128]{2,0,1:T(8,128)(2,1)S(1)}, u32[]{:S(2)}, u32[]{:S(2)}) async-start(bf16[128,16,128]{2,0,1:T(8,128)(2,1)} %bitcast.132), calls=%async_computation | async-start | bytes 1048576 | tf_op jit(solution)/shard_map/all_to_all | solution.py:78
  23.9 18.3 %all-to-all-start.2 = ((bf16[128,16,128]{2,0,1:T(8,128)(2,1)}), bf16[128,16,128]{2,0,1:T(8,128)(2,1)S(1)}, u32[]{:S(2)}, u32[]{:S(2)}) async-start(bf16[128,16,128]{2,0,1:T(8,128)(2,1)} %bitcast.155), calls=%async_computation.2 | async-start | bytes 1048576 | tf_op jit(solution)/shard_map/all_to_all | solution.py:80
  42.2 18.4 %all-to-all-start.1 = ((bf16[128,16,128]{2,0,1:T(8,128)(2,1)}), bf16[128,16,128]{2,0,1:T(8,128)(2,1)}, u32[]{:S(2)}, u32[]{:S(2)}) async-start(bf16[128,16,128]{2,0,1:T(8,128)(2,1)} %bitcast.154), calls=%async_computation.1 | async-start | bytes 1048576 | tf_op jit(solution)/shard_map/all_to_all | solution.py:79
  48.2 13.8 %copy-start.6 = (s32[32,5]{0,1:T(8,128)}, s32[32,5]{0,1:T(8,128)S(1)}, u32[]{:S(2)}) copy-start(s32[32,5]{0,1:T(8,128)S(1)} %reduce-window.9) | copy-start | bytes 1924
  49.3 13.8 %copy-start.5 = (f32[128]{0:T(128)S(1)}, f32[128]{0:T(128)}, u32[]{:S(2)}) copy-start(f32[128]{0:T(128)} %param.24) | copy-start | bytes 1540
  49.3 13.8 %copy-start.13 = (f32[2]{0:T(128)S(1)}, f32[2]{0:T(128)}, u32[]{:S(2)}) copy-start(f32[2]{0:T(128)} %param.23) | copy-start | bytes 28
  51.8 11.3 %copy-start.2 = (bf16[2,512,2,2,64]{1,4,3,2,0:T(8,128)(2,1)S(1)}, bf16[2,512,2,2,64]{1,4,3,2,0:T(8,128)(2,1)}, u32[]{:S(2)}) copy-start(bf16[2,512,2,2,64]{1,4,3,2,0:T(8,128)(2,1)} %copy.57) | copy-start | bytes 1572868
  63.1 35.9 %slice-start = ((s32[32,5]{0,1:T(8,128)}), s32[32,4]{0,1:T(4,128)S(1)}, s32[]{:S(2)}) async-start(s32[32,5]{0,1:T(8,128)} %copy-done.6), calls=%async_computation.6 | async-start | bytes 4096 | tf_op jit(solution)/shard_map/slice.1
  72.0 4.0 %copy-start.3 = (bf16[1024,2,128]{0,2,1:T(8,128)(2,1)S(1)}, bf16[1024,2,128]{0,2,1:T(8,128)(2,1)}, u32[]{:S(2)}) copy-start(bf16[1024,2,128]{0,2,1:T(8,128)(2,1)} %get-tuple-element.204) | copy-start | bytes 1572868 | tf_op jit(solution)/shard_map/while
  86.8 4.0 %copy-start.3 = (bf16[1024,2,128]{0,2,1:T(8,128)(2,1)S(1)}, bf16[1024,2,128]{0,2,1:T(8,128)(2,1)}, u32[]{:S(2)}) copy-start(bf16[1024,2,128]{0,2,1:T(8,128)(2,1)} %get-tuple-element.204) | copy-start | bytes 1572868 | tf_op jit(solution)/shard_map/while
  95.1 18.2 %all-to-all-start.3 = ((bf16[1024,2,128]{2,1,0:T(2,128)(2,1)}), bf16[1024,2,128]{2,1,0:T(2,128)(2,1)S(1)}, u32[]{:S(2)}, u32[]{:S(2)}) async-start(bf16[1024,2,128]{2,1,0:T(2,128)(2,1)} %copy.59), calls=%async_computation.3 | async-start | bytes 1048576 | tf_op jit(solution)/shard_map/all_to_all | solution.py:83
  113.6 4.8 %copy-start.4 = (bf16[1,128,2048]{2,1,0:T(8,128)(2,1)S(1)}, bf16[1,128,2048]{2,1,0:T(8,128)(2,1)}, u32[]{:S(2)}) copy-start(bf16[1,128,2048]{2,1,0:T(8,128)(2,1)} %param.25) | copy-start | bytes 1572868
  113.6 4.8 %copy-start.7 = (f32[2048]{0:T(1024)S(1)}, f32[2048]{0:T(1024)}, u32[]{:S(2)}) copy-start(f32[2048]{0:T(1024)} %param.27) | copy-start | bytes 24580
  113.7 5.2 %copy-start.8 = (f32[2048]{0:T(1024)S(1)}, f32[2048]{0:T(1024)}, u32[]{:S(2)}) copy-start(f32[2048]{0:T(1024)} %param.28) | copy-start | bytes 24580
  125.5 76.3 %copy-start.12 = (bf16[1,2048,512]{2,1,0:T(8,128)(2,1)S(1)}, bf16[1,2048,512]{2,1,0:T(8,128)(2,1)}, u32[]{:S(2)}) copy-start(bf16[1,2048,512]{2,1,0:T(8,128)(2,1)} %param.32) | copy-start | bytes 6291460
  200.1 1.7 copy-start.1
  212.9 4.0 %copy-start.11 = (f32[1,128,4]{1,2,0:T(4,128)S(1)}, f32[1,128,4]{1,2,0:T(4,128)}, u32[]{:S(2)}) copy-start(f32[1,128,4]{1,2,0:T(4,128)} %param.31) | copy-start | bytes 6148
  212.9 75.3 %all-to-all-start.5 = ((bf16[32,24,2048]{2,1,0:T(8,128)(2,1)}), bf16[32,24,2048]{2,1,0:T(8,128)(2,1)}, u32[]{:S(2)}, u32[]{:S(2)}) async-start(bf16[32,24,2048]{2,1,0:T(8,128)(2,1)} %bitcast.149), calls=%async_computation.5 | async-start | bytes 6291456 | tf_op jit(solution)/shard_map/all_to_all | solution.py:121
  306.8 4.4 %copy-start.9 = (f32[2048]{0:T(1024)S(1)}, f32[2048]{0:T(1024)}, u32[]{:S(2)}) copy-start(f32[2048]{0:T(1024)} %param.29) | copy-start | bytes 24580
where the time goes:
time: 315 us; the launch traced here: 313 us
  waiting for transfers between devices  110 us (35%)
  blocking collectives  74.6 us (24%)
  local copies, waits for them, and re-layouts  44.7 us (14%)
  matrix products  38.3 us (12%)
  starting transfers between devices  22.7 us (7%)
  other arithmetic  21.5 us (7%)
    all_to_all x1, blocking collectives, local(): lax.all_to_all(outgoing, ('sp', 'dp'), split_axis=0, concat_axis=0, tiled...  74.6 us
    all_to_all x1, waiting for transfers between devices, local(): lax.all_to_all(results, ('sp', 'dp'), split_axis=0, concat_axis=0, tiled=...  69.1 us
    sub x2, matrix products, one_block(): exponent = jnp.exp(scores - maxima)  14.3 us
    all_to_all x1, waiting for transfers between devices, local(): lax.all_to_all(value_vectors[0], 'sp', split_axis=1, concat_axis=0, tiled...  12.7 us
    all_to_all x1, waiting for transfers between devices, local(): lax.all_to_all(queries[0], 'sp', split_axis=1, concat_axis=0, tiled=True)  12.5 us
    dot_general x2, matrix products, feed_forward(): jnp.dot(hidden, down_w, preferred_element_type=jnp.float32)  12.5 us
    unnamed x31, local copies, waits for them, and re-layouts  8.84 us
    div x2, other arithmetic, one_block(): softmax_both = exponent / jnp.sum(exponent, axis=-1, keepdims=True)  7.91 us
  transfers between devices with their start and end apart: 5, of which 5 were waited for; matrix products, arithmetic and copies ran while one was open for 6% of the time, Pallas kernels for 0%

commit v1 on v0

--- a/solution.py
+++ b/solution.py
@@ -75,7 +75,12 @@
     shared_down,
 ):
     query_heads, key_heads, value_heads = (
-        lax.all_to_all(queries[0], "sp", split_axis=1, concat_axis=0, tiled=True),
+        jnp.concatenate(
+            lax.all_to_all(
+                jnp.stack(jnp.split(queries[0], lax.axis_size("sp"), axis=1)), "sp", 0, 0
+            ),
+            axis=0,
+        ),
         lax.all_to_all(key_vectors[0], "sp", split_axis=1, concat_axis=0, tiled=True),
         lax.all_to_all(value_vectors[0], "sp", split_axis=1, concat_axis=0, tiled=True),
     )

time: 315 us -> 326 us (1.035)
  local copies, waits for them, and re-layouts: 44.7 us -> 58.9 us
    unnamed x31 -> x41, local copies, waits for them, and re-layouts: 8.84 us -> 19.8 us
    another operation x2 -> x4, local copies, waits for them, and re-layouts: 0.01 us -> 4.58 us  [the longest x1 2.93 us: attend_heads(): query_heads.reshape(block_count, block_rows, head_count, 2, head_size)]
  transfers between devices with their start and end apart: 5 -> 5, of which waited for: 5 -> 5; matrix products, arithmetic and copies ran while one was open for 6% -> 7% of each run, Pallas kernels for 0% -> 0%
where the time goes in v1:
time: 326 us; the launch traced here: 325 us
  waiting for transfers between devices  107 us (33%)
  blocking collectives  74.6 us (23%)
  local copies, waits for them, and re-layouts  58.9 us (18%)
  matrix products  38.3 us (12%)
  starting transfers between devices  22.7 us (7%)
  other arithmetic  21.5 us (7%)
    all_to_all x1, blocking collectives, local(): lax.all_to_all(outgoing, ('sp', 'dp'), split_axis=0, concat_axis=0, tiled...  74.6 us
    all_to_all x1, waiting for transfers between devices, local(): lax.all_to_all(results, ('sp', 'dp'), split_axis=0, concat_axis=0, tiled=...  69.1 us
    unnamed x41, local copies, waits for them, and re-layouts  19.8 us
    sub x2, matrix products, one_block(): exponent = jnp.exp(scores - maxima)  14.3 us
    all_to_all x1, waiting for transfers between devices, local(): lax.all_to_all(value_vectors[0], 'sp', split_axis=1, concat_axis=0, tiled...  12.7 us
    all_to_all x1, waiting for transfers between devices, local(): lax.all_to_all(jnp.stack(jnp.split(queries[0], lax.axis_size('sp'), axis=...  12.5 us
    dot_general x2, matrix products, feed_forward(): jnp.dot(hidden, down_w, preferred_element_type=jnp.float32)  12.5 us
    div x2, other arithmetic, one_block(): softmax_both = exponent / jnp.sum(exponent, axis=-1, keepdims=True)  7.91 us
  transfers between devices with their start and end apart: 5, of which 5 were waited for; matrix products, arithmetic and copies ran while one was open for 7% of the time, Pallas kernels for 0%

profile of v1, /device:TPU:0, one launch (start us, length us, event | category | flops | bytes accessed | tf_op | source)
XLA Modules:
  0.0 324.5 jit_solution(2665413772470610421)
XLA Ops:
  13.3 7.3 %all-to-all-start = ((bf16[8,128,2,128]{3,2,1,0:T(2,128)(2,1)}), bf16[8,128,2,128]{3,2,1,0:T(2,128)(2,1)S(1)}, u32[]{:S(2)}, u32[]{:S(2)}) async-start(bf16[8,128,2,128]{3,2,1,0:T(2,128)(2,1)} %fusion.62), calls=%async_computation | async-start | bytes 1048576 | tf_op jit(solution)/shard_map/all_to_all | solution.py:79
  22.6 12.5 %all-to-all-done = bf16[8,128,2,128]{3,2,1,0:T(2,128)(2,1)S(1)} async-done(((bf16[8,128,2,128]{3,2,1,0:T(2,128)(2,1)}), bf16[8,128,2,128]{3,2,1,0:T(2,128)(2,1)S(1)}, u32[]{:S(2)}, u32[]{:S(2)}) %all-to-all-start) | async-done | bytes 524320 | tf_op jit(solution)/shard_map/all_to_all | solution.py:79
  35.1 3.6 %all-to-all-start.2 = ((bf16[128,16,128]{2,0,1:T(8,128)(2,1)}), bf16[128,16,128]{2,0,1:T(8,128)(2,1)S(1)}, u32[]{:S(2)}, u32[]{:S(2)}) async-start(bf16[128,16,128]{2,0,1:T(8,128)(2,1)} %bitcast.178), calls=%async_computation.2 | async-start | bytes 1048576 | tf_op jit(solution)/shard_map/all_to_all | solution.py:85
  40.7 12.7 %all-to-all-done.2 = bf16[128,16,128]{2,0,1:T(8,128)(2,1)S(1)} async-done(((bf16[128,16,128]{2,0,1:T(8,128)(2,1)}), bf16[128,16,128]{2,0,1:T(8,128)(2,1)S(1)}, u32[]{:S(2)}, u32[]{:S(2)}) %all-to-all-start.2) | async-done | bytes 524320 | tf_op jit(solution)/shard_map/all_to_all | solution.py:85
  53.4 4.1 %all-to-all-start.1 = ((bf16[128,16,128]{2,0,1:T(8,128)(2,1)}), bf16[128,16,128]{2,0,1:T(8,128)(2,1)}, u32[]{:S(2)}, u32[]{:S(2)}) async-start(bf16[128,16,128]{2,0,1:T(8,128)(2,1)} %bitcast.177), calls=%async_computation.1 | async-start | bytes 1048576 | tf_op jit(solution)/shard_map/all_to_all | solution.py:84
  59.4 2.9 reshape.172
  62.3 2.3 copy.55
  67.1 4.7 %all-to-all-done.1 = bf16[128,16,128]{2,0,1:T(8,128)(2,1)} async-done(((bf16[128,16,128]{2,0,1:T(8,128)(2,1)}), bf16[128,16,128]{2,0,1:T(8,128)(2,1)}, u32[]{:S(2)}, u32[]{:S(2)}) %all-to-all-start.1) | async-done | bytes 524320 | tf_op jit(solution)/shard_map/all_to_all | solution.py:84
  74.3 29.6 %while.11 = (s32[]{:T(128)}, bf16[2,512,2,128]{3,1,0,2:T(8,128)(2,1)}, s32[2]{0:T(128)S(1)}, bf16[2,512,2,2,64]{1,4,3,2,0:T(8,128)(2,1)S(1)}, bf16[1024,2,2,64]{...) while((s32[]{:T(128)}, ...), condition=%wide.region_4.5_spmd.clone, body=%wide.region_0.4_spmd.clone.sunk | while | flops 551684608 | bytes 40408232 | solution.py:53
  76.0 7.1 %fusion.107 = (f32[2,2,512]{2,1,0:T(2,128)S(1)}, f32[2,2,512,1024]{3,2,1,0:T(8,128)}) fusion(pred[512,1024]{1,0:T(8,128)(4,1)S(1)} %iota_compare_fusion.4, bf16[1024,2,2,64]{0,3,2,1:T(8,128)(2,1)} %get-tuple-element.202, bf16[2,512,2,2,64]{1,4,3,2,0:T(8,128)(2,1)S(1)} %get-tuple-element.201, s32[]{:T(128)} %get-tuple-element.188), kind=kOutput, calls=%fused_computation.117.clone.1 | convolution fusion | flops 276825088 | bytes 9707524 | tf_op jit(solution)/shard_map/while/body/eval_jaxpr/sub | solution.py:43
  83.2 4.0 %broadcast_divide_fusion.2 = f32[2,2,512,1024]{3,2,1,0:T(8,128)S(1)} fusion(f32[2,2,512,1024]{3,2,1,0:T(8,128)} %get-tuple-element.174, f32[2,2,512]{2,1,0:T(2,128)S(1)} %get-tuple-element.175), kind=kLoop, calls=%fused_computation.14.clone.1 | loop fusion | flops 2097152 | bytes 16785408 | tf_op jit(solution)/shard_map/while/body/eval_jaxpr/div | solution.py:44
  90.8 7.1 %fusion.107 = (f32[2,2,512]{2,1,0:T(2,128)S(1)}, f32[2,2,512,1024]{3,2,1,0:T(8,128)}) fusion(pred[512,1024]{1,0:T(8,128)(4,1)S(1)} %iota_compare_fusion.4, bf16[1024,2,2,64]{0,3,2,1:T(8,128)(2,1)} %get-tuple-element.202, bf16[2,512,2,2,64]{1,4,3,2,0:T(8,128)(2,1)S(1)} %get-tuple-element.201, s32[]{:T(128)} %get-tuple-element.188), kind=kOutput, calls=%fused_computation.117.clone.1 | convolution fusion | flops 276825088 | bytes 9707524 | tf_op jit(solution)/shard_map/while/body/eval_jaxpr/sub | solution.py:43
  98.0 4.0 %broadcast_divide_fusion.2 = f32[2,2,512,1024]{3,2,1,0:T(8,128)S(1)} fusion(f32[2,2,512,1024]{3,2,1,0:T(8,128)} %get-tuple-element.174, f32[2,2,512]{2,1,0:T(2,128)S(1)} %get-tuple-element.175), kind=kLoop, calls=%fused_computation.14.clone.1 | loop fusion | flops 2097152 | bytes 16785408 | tf_op jit(solution)/shard_map/while/body/eval_jaxpr/div | solution.py:44
  103.9 2.4 copy.57
  106.2 3.6 %all-to-all-start.3 = ((bf16[1024,2,128]{2,1,0:T(2,128)(2,1)}), bf16[1024,2,128]{2,1,0:T(2,128)(2,1)S(1)}, u32[]{:S(2)}, u32[]{:S(2)}) async-start(bf16[1024,2,128]{2,1,0:T(2,128)(2,1)} %copy.57), calls=%async_computation.3 | async-start | bytes 1048576 | tf_op jit(solution)/shard_map/all_to_all | solution.py:88
  110.2 2.6 scatter_custom_fusion
  112.9 3.8 %scatter_custom_fusion.1 = bf16[768]{0:T(1024)(128)(2,1)S(1)} fusion(s32[512]{0:T(512)S(1)} %bitcast.190, bf16[512]{0:T(512)(128)(2,1)S(1)} %broadcast.140, bf16[]{:T(256)} %constant.60.clone.1), kind=kCustom, calls=%fused_computation.109 | custom fusion | bytes 1538 | tf_op jit(solution)/shard_map/scatter | solution.py:116
  116.8 7.6 %all-to-all-done.3 = bf16[1024,2,128]{2,1,0:T(2,128)(2,1)S(1)} async-done(((bf16[1024,2,128]{2,1,0:T(2,128)(2,1)}), bf16[1024,2,128]{2,1,0:T(2,128)(2,1)S(1)}, u32[]{:S(2)}, u32[]{:S(2)}) %all-to-all-start.3) | async-done | bytes 524320 | tf_op jit(solution)/shard_map/all_to_all | solution.py:88
  124.8 4.8 %multiply_reduce_fusion.3 = (f32[128]{0:T(128)S(1)}, f32[128,2048]{1,0:T(8,128)S(1)}) fusion(bf16[128,2048]{0,1:T(8,128)(2,1)S(1)} %bitcast.172, bf16[2048,2048]{1,0:T(8,128)(2,1)} %param.26), kind=kOutput, calls=%fused_computation.61 | convolution fusion | flops 1074265984 | bytes 9961984 | tf_op jit(solution)/shard_map/dot_general | solution.py:91
  130.2 4.3 %gather_fusion = bf16[768,2048]{1,0:T(8,128)(2,1)} fusion(bf16[128,2048]{1,0:T(8,128)(2,1)S(1)} %fusion.47, s32[1024]{0:T(1024)S(1)} %pad_clamp_fusion.1), kind=kCustom, calls=%fused_computation | custom fusion | bytes 6294528 | tf_op jit(solution)/shard_map/gather | solution.py:118
  134.5 2.2 broadcast_multiply_fusion
  136.7 74.6 %all_to_all.63 = bf16[32,24,2048]{2,1,0:T(8,128)(2,1)S(1)} all-to-all(bf16[32,24,2048]{2,1,0:T(8,128)(2,1)S(1)} %broadcast_multiply_fusion), channel_id=1, replica_groups=mesh['sp'=8,'dp'=4] {'sp','dp'}, dimensions={0} | all-to-all | bytes 6291456 | tf_op jit(solution)/shard_map/all_to_all | solution.py:122
  213.0 2.9 fusion.40
  215.9 8.1 %convolution_convert_fusion = bf16[768,2048]{1,0:T(8,128)(2,1)} fusion(bf16[1,512,2048]{2,1,0:T(8,128)(2,1)S(1)} %copy-done, f32[768,512]{1,0:T(8,128)} %fusion.40, bf16[768,2048]{1,0:T(8,128)(2,1)} %bitcast.175, bf16[1,2048,512]{2,1,0:T(8,128)(2,1)} %param.33), kind=kOutput, calls=%fused_computation.38 | convolution fusion | flops 3225157632 | bytes 12058624 | tf_op jit(solution)/shard_map/dot_general | solution.py:21
  224.1 4.0 %all-to-all-start.5 = ((bf16[32,24,2048]{2,1,0:T(8,128)(2,1)}), bf16[32,24,2048]{2,1,0:T(8,128)(2,1)}, u32[]{:S(2)}, u32[]{:S(2)}) async-start(bf16[32,24,2048]{2,1,0:T(8,128)(2,1)} %bitcast.173), calls=%async_computation.5 | async-start | bytes 6291456 | tf_op jit(solution)/shard_map/all_to_all | solution.py:126
  228.2 2.0 fusion.86
  230.3 69.1 %all-to-all-done.5 = bf16[32,24,2048]{2,1,0:T(8,128)(2,1)} async-done(((bf16[32,24,2048]{2,1,0:T(8,128)(2,1)}), bf16[32,24,2048]{2,1,0:T(8,128)(2,1)}, u32[]{:S(2)}, u32[]{:S(2)}) %all-to-all-start.5) | async-done | bytes 3145760 | tf_op jit(solution)/shard_map/all_to_all | solution.py:126
  299.3 7.5 %gather_fusion.1 = bf16[512,2048]{1,0:T(8,128)(2,1)} fusion(bf16[768,2048]{1,0:T(8,128)(2,1)} %bitcast.29, s32[1024]{0:T(1024)S(1)} %pad_clamp_fusion), kind=kCustom, calls=%fused_computation.1 | custom fusion | bytes 4196352 | tf_op jit(solution)/shard_map/gather | solution.py:127
  306.8 4.8 %reshape.138 = f32[128,4,2048]{2,1,0:T(4,128)} reshape(bf16[512,2048]{1,0:T(8,128)(2,1)} %gather_fusion.1) | data formatting | bytes 6291456 | tf_op jit(solution)/shard_map/convert_element_type | solution.py:129
  311.6 6.3 %multiply_reduce_fusion.1 = f32[128,2048]{1,0:T(8,128)} fusion(f32[128,4,2048]{2,1,0:T(4,128)} %reshape.138, f32[128,4]{1,0:T(8,128)S(1)} %copy.64), kind=kLoop, calls=%fused_computation.37 | loop fusion | flops 1835008 | bytes 5244928 | tf_op jit(solution)/shard_map/reduce_sum | solution.py:128
  317.9 4.3 %multiply_reduce_fusion.2 = (f32[128]{0:T(128)S(1)}, f32[128,2048]{1,0:T(8,128)}) fusion(f32[128,2048]{1,0:T(8,128)} %multiply_reduce_fusion.1, bf16[512,2048]{1,0:T(8,128)(2,1)} %param.37, bf16[128,2048]{1,0:T(8,128)(2,1)S(1)} %fusion.47, bf16[2048,512]{1,0:T(8,128)(2,1)} %param.36, f32[128,512]{1,0:T(8,128)S(1)} %fusion.86), kind=kOutput, calls=%fused_computation.60 | convolution fusion | flops 538574720 | bytes 7078400 | tf_op jit(solution)/shard_map/dot_general | solution.py:21
  322.3 2.2 fusion.52
  (94 shorter events, 33.1 us)
Async XLA Ops:
  0.0 215.9 %copy-start = (bf16[1,512,2048]{2,1,0:T(8,128)(2,1)S(1)}, bf16[1,512,2048]{2,1,0:T(8,128)(2,1)}, u32[]{:S(2)}) copy-start(bf16[1,512,2048]{2,1,0:T(8,128)(2,1)} %param.34) | copy-start | bytes 6291460
  0.0 57.6 %copy-start.12 = (s32[1,128,4]{1,2,0:T(4,128)S(1)}, s32[1,128,4]{1,2,0:T(4,128)}, u32[]{:S(2)}) copy-start(s32[1,128,4]{1,2,0:T(4,128)} %param.30) | copy-start | bytes 6148
  13.3 21.8 %all-to-all-start = ((bf16[8,128,2,128]{3,2,1,0:T(2,128)(2,1)}), bf16[8,128,2,128]{3,2,1,0:T(2,128)(2,1)S(1)}, u32[]{:S(2)}, u32[]{:S(2)}) async-start(bf16[8,128,2,128]{3,2,1,0:T(2,128)(2,1)} %fusion.62), calls=%async_computation | async-start | bytes 1048576 | tf_op jit(solution)/shard_map/all_to_all | solution.py:79
  35.1 24.3 %copy-start.2 = (bf16[8,128,2,128]{3,2,1,0:T(2,128)(2,1)}, bf16[8,128,2,128]{3,2,1,0:T(2,128)(2,1)S(1)}, u32[]{:S(2)}) copy-start(bf16[8,128,2,128]{3,2,1,0:T(2,128)(2,1)S(1)} %all-to-all-done) | copy-start | bytes 1572868
  35.1 18.3 %all-to-all-start.2 = ((bf16[128,16,128]{2,0,1:T(8,128)(2,1)}), bf16[128,16,128]{2,0,1:T(8,128)(2,1)S(1)}, u32[]{:S(2)}, u32[]{:S(2)}) async-start(bf16[128,16,128]{2,0,1:T(8,128)(2,1)} %bitcast.178), calls=%async_computation.2 | async-start | bytes 1048576 | tf_op jit(solution)/shard_map/all_to_all | solution.py:85
  53.4 6.0 %copy-start.3 = (bf16[128,16,128]{2,0,1:T(8,128)(2,1)}, bf16[128,16,128]{2,0,1:T(8,128)(2,1)S(1)}, u32[]{:S(2)}) copy-start(bf16[128,16,128]{2,0,1:T(8,128)(2,1)S(1)} %all-to-all-done.2) | copy-start | bytes 1572868
  53.4 18.4 %all-to-all-start.1 = ((bf16[128,16,128]{2,0,1:T(8,128)(2,1)}), bf16[128,16,128]{2,0,1:T(8,128)(2,1)}, u32[]{:S(2)}, u32[]{:S(2)}) async-start(bf16[128,16,128]{2,0,1:T(8,128)(2,1)} %bitcast.177), calls=%async_computation.1 | async-start | bytes 1048576 | tf_op jit(solution)/shard_map/all_to_all | solution.py:84
  59.4 13.8 %copy-start.8 = (s32[32,5]{0,1:T(8,128)}, s32[32,5]{0,1:T(8,128)S(1)}, u32[]{:S(2)}) copy-start(s32[32,5]{0,1:T(8,128)S(1)} %reduce-window.9) | copy-start | bytes 1924
  62.3 12.0 %copy-start.7 = (f32[128]{0:T(128)S(1)}, f32[128]{0:T(128)}, u32[]{:S(2)}) copy-start(f32[128]{0:T(128)} %param.24) | copy-start | bytes 1540
  62.3 12.0 %copy-start.15 = (f32[2]{0:T(128)S(1)}, f32[2]{0:T(128)}, u32[]{:S(2)}) copy-start(f32[2]{0:T(128)} %param.23) | copy-start | bytes 28
  64.7 9.6 %copy-start.4 = (bf16[2,512,2,2,64]{1,4,3,2,0:T(8,128)(2,1)S(1)}, bf16[2,512,2,2,64]{1,4,3,2,0:T(8,128)(2,1)}, u32[]{:S(2)}) copy-start(bf16[2,512,2,2,64]{1,4,3,2,0:T(8,128)(2,1)} %copy.55) | copy-start | bytes 1572868
  74.3 35.9 %slice-start = ((s32[32,5]{0,1:T(8,128)}), s32[32,4]{0,1:T(4,128)S(1)}, s32[]{:S(2)}) async-start(s32[32,5]{0,1:T(8,128)} %copy-done.8), calls=%async_computation.6 | async-start | bytes 4096 | tf_op jit(solution)/shard_map/slice.1
  83.2 4.0 %copy-start.5 = (bf16[1024,2,128]{0,2,1:T(8,128)(2,1)S(1)}, bf16[1024,2,128]{0,2,1:T(8,128)(2,1)}, u32[]{:S(2)}) copy-start(bf16[1024,2,128]{0,2,1:T(8,128)(2,1)} %get-tuple-element.204) | copy-start | bytes 1572868 | tf_op jit(solution)/shard_map/while
  98.0 4.0 %copy-start.5 = (bf16[1024,2,128]{0,2,1:T(8,128)(2,1)S(1)}, bf16[1024,2,128]{0,2,1:T(8,128)(2,1)}, u32[]{:S(2)}) copy-start(bf16[1024,2,128]{0,2,1:T(8,128)(2,1)} %get-tuple-element.204) | copy-start | bytes 1572868 | tf_op jit(solution)/shard_map/while
  106.2 18.2 %all-to-all-start.3 = ((bf16[1024,2,128]{2,1,0:T(2,128)(2,1)}), bf16[1024,2,128]{2,1,0:T(2,128)(2,1)S(1)}, u32[]{:S(2)}, u32[]{:S(2)}) async-start(bf16[1024,2,128]{2,1,0:T(2,128)(2,1)} %copy.57), calls=%async_computation.3 | async-start | bytes 1048576 | tf_op jit(solution)/shard_map/all_to_all | solution.py:88
  124.8 4.8 %copy-start.6 = (bf16[1,128,2048]{2,1,0:T(8,128)(2,1)S(1)}, bf16[1,128,2048]{2,1,0:T(8,128)(2,1)}, u32[]{:S(2)}) copy-start(bf16[1,128,2048]{2,1,0:T(8,128)(2,1)} %param.25) | copy-start | bytes 1572868
  124.8 4.8 %copy-start.9 = (f32[2048]{0:T(1024)S(1)}, f32[2048]{0:T(1024)}, u32[]{:S(2)}) copy-start(f32[2048]{0:T(1024)} %param.27) | copy-start | bytes 24580
  124.8 5.2 %copy-start.10 = (f32[2048]{0:T(1024)S(1)}, f32[2048]{0:T(1024)}, u32[]{:S(2)}) copy-start(f32[2048]{0:T(1024)} %param.28) | copy-start | bytes 24580
  136.7 76.3 %copy-start.14 = (bf16[1,2048,512]{2,1,0:T(8,128)(2,1)S(1)}, bf16[1,2048,512]{2,1,0:T(8,128)(2,1)}, u32[]{:S(2)}) copy-start(bf16[1,2048,512]{2,1,0:T(8,128)(2,1)} %param.32) | copy-start | bytes 6291460
  211.3 1.7 copy-start.1
  224.1 4.0 %copy-start.13 = (f32[1,128,4]{1,2,0:T(4,128)S(1)}, f32[1,128,4]{1,2,0:T(4,128)}, u32[]{:S(2)}) copy-start(f32[1,128,4]{1,2,0:T(4,128)} %param.31) | copy-start | bytes 6148
  224.1 75.3 %all-to-all-start.5 = ((bf16[32,24,2048]{2,1,0:T(8,128)(2,1)}), bf16[32,24,2048]{2,1,0:T(8,128)(2,1)}, u32[]{:S(2)}, u32[]{:S(2)}) async-start(bf16[32,24,2048]{2,1,0:T(8,128)(2,1)} %bitcast.173), calls=%async_computation.5 | async-start | bytes 6291456 | tf_op jit(solution)/shard_map/all_to_all | solution.py:126
  317.9 4.4 %copy-start.11 = (f32[2048]{0:T(1024)S(1)}, f32[2048]{0:T(1024)}, u32[]{:S(2)}) copy-start(f32[2048]{0:T(1024)} %param.29) | copy-start | bytes 24580
